TPU v7x, 128 devices: a whole 4x4x4 slice. The times are simulated.
128 devices in a mesh: kv: 16 (over z, y), tp: 8 (over x, core).
Axes of the slice: x: 4, y: 4, z: 4, core: 2. Of those that a mesh axis runs over, the one named last changes fastest.
Arguments:
- tokens: bfloat16 [512, 4096], P(None, ('kv', 'tp')), may hold values from -60 to 60
- past_state: float32 [512, 16, 128, 128], P('kv', 'tp'), may hold values from -4 to 4
- pre_gain: float32 [4096], replicated, may hold values from 0.1 to 1.9
- pre_gate: bfloat16 [4096, 11264], P(None, ('kv', 'tp')), may hold values from -0.09375 to 0.09375
- pre_up: bfloat16 [4096, 11264], P(None, ('kv', 'tp')), may hold values from -0.09375 to 0.09375
- pre_down: bfloat16 [11264, 4096], P(('kv', 'tp')), may hold values from -0.21875 to 0.21875
- mix_gain: float32 [4096], replicated, may hold values from 0.1 to 1.9
- query_weight: bfloat16 [4096, 2048], P('kv', 'tp'), may hold values from -0.09375 to 0.09375
- forget_weight: bfloat16 [4096, 2048], P('kv', 'tp'), may hold values from -0.09375 to 0.09375
- value_weight: bfloat16 [4096, 2048], P('kv', 'tp'), may hold values from -0.09375 to 0.09375
- output_gate_weight: bfloat16 [4096, 2048], P('kv', 'tp'), may hold values from -0.09375 to 0.09375
- forget_floor: float32 [2048], P('tp'), may hold values from 0.02 to 0.9
- head_gain: float32 [128], replicated, may hold values from 0.1 to 1.9
- proj_out: bfloat16 [2048, 4096], P('tp', 'kv'), may hold values from -0.125 to 0.125
- post_gain: float32 [4096], replicated, may hold values from 0.1 to 1.9
- post_gate: bfloat16 [4096, 11264], P(None, ('kv', 'tp')), may hold values from -0.09375 to 0.09375
- post_up: bfloat16 [4096, 11264], P(None, ('kv', 'tp')), may hold values from -0.09375 to 0.09375
- post_down: bfloat16 [11264, 4096], P(('kv', 'tp')), may hold values from -0.21875 to 0.21875
Outputs:
- result: bfloat16 [512, 4096], P(None, ('kv', 'tp'))
- new_state: float32 [512, 16, 128, 128], P('kv', 'tp')
All inputs are finite; a program needn't handle non-finite values.
Results may differ from a plain program's by a relative error of at most 0.014.
Values may be sent and summed in bfloat16 or wider, within the bound.
No kernel may reach another device: no remote copies, remote signals or barrier semaphores. Data moves between devices by JAX's collectives and lax.ppermute only.
A program may use at most 128 MiB of HBM per device.

v0:
```python
import functools

import jax
import jax.numpy as jnp
from jax import lax
from jax.sharding import Mesh
from jax.sharding import PartitionSpec as P

D = 4096
KV_TP = ("kv_0", "kv_1", "tp_0", "tp_1")
TP = ("tp_0", "tp_1")
KV = ("kv_0", "kv_1")


epsilon = 1e-06


def copy_for_each(value, axis):
    copies = jnp.broadcast_to(value, (lax.axis_size(axis), *value.shape))
    return lax.all_to_all(copies, axis, split_axis=0, concat_axis=0, tiled=True)


def in_order(pieces, dim):
    pieces = jnp.moveaxis(pieces, 0, dim)
    dims = pieces.shape
    return pieces.reshape(*dims[:dim], dims[dim] * dims[dim + 1], *dims[dim + 2 :])


def gather_axes(value, axes, dim):
    far, near = axes
    pieces = copy_for_each(copy_for_each(value, far), near)
    return in_order(pieces.swapaxes(0, 1).reshape(-1, *value.shape), dim)


def split_up(value, dim, devices):
    dims = value.shape
    pieces = value.reshape(*dims[:dim], devices, dims[dim] // devices, *dims[dim + 1 :])
    return jnp.moveaxis(pieces, dim, 0)


def sum_at_owner(value, axis, dim):
    devices = lax.axis_size(axis)
    pieces = lax.all_to_all(split_up(value, dim, devices), axis, 0, 0, tiled=True)
    return jnp.sum(pieces.astype(jnp.float32), axis=0)


def summed_rows(value, axes, dim):
    far, near = axes
    pieces = split_up(value, dim, lax.axis_size(far))
    nearer = sum_at_owner(pieces, near, dim + 1)
    arrived = lax.all_to_all(
        nearer.astype(jnp.bfloat16), far, split_axis=0, concat_axis=0, tiled=True
    )
    return arrived.astype(jnp.float32).sum(axis=0)


def collect(value, axis, dim):
    pieces = copy_for_each(value, axis)
    return in_order(pieces, dim)


def over_axes(value, axes):
    return functools.reduce(lax.psum, axes, value)


def half_inputs(activations, gain, w_gate, w_up):
    piece_float = gather_axes(activations, (("kv_0", "kv_1", "tp_0"), "tp_1"), 1).astype(
        jnp.float32
    )
    normed = (piece_float * gain).astype(jnp.bfloat16)
    gate_acc = jnp.dot(normed, w_gate, preferred_element_type=jnp.float32)
    up_acc = jnp.dot(normed, w_up, preferred_element_type=jnp.float32)
    squares = jnp.sum(piece_float * piece_float, axis=1)
    row_scale = lax.rsqrt(squares / D + epsilon)[:, None]
    return (jax.nn.silu(row_scale * gate_acc) * (row_scale * up_acc)).astype(jnp.bfloat16)


def down_sum(hidden, w_down):
    return summed_rows(
        jnp.dot(hidden, w_down, preferred_element_type=jnp.float32).astype(jnp.bfloat16),
        (("kv_0", "kv_1", "tp_0"), "tp_1"),
        1,
    )


def per_device(
    tokens,
    past_state,
    pre_gain,
    pre_gate,
    pre_up,
    pre_down,
    mix_gain,
    query_weight,
    forget_weight,
    value_weight,
    output_gate_weight,
    forget_floor,
    head_gain,
    proj_out,
    post_gain,
    post_gate,
    post_up,
    post_down,
):
    hidden = half_inputs(tokens, pre_gain, pre_gate, pre_up)
    after_first = (tokens.astype(jnp.float32) + 0.5 * down_sum(hidden, pre_down)).astype(
        jnp.bfloat16
    )
    block_rows = collect(after_first, TP, 1)
    block_width = block_rows.shape[1]
    block_float = block_rows.astype(jnp.float32)
    block_gain = lax.dynamic_slice_in_dim(
        mix_gain, lax.axis_index(KV) * block_width, block_width, 0
    )
    squares = over_axes(jnp.sum(block_float * block_float, axis=1), KV)
    normed = (block_float * block_gain).astype(jnp.bfloat16)
    own_rows = past_state.shape[0]
    weight_list = (query_weight, forget_weight, value_weight, output_gate_weight)
    projected = sum_at_owner(
        jnp.concatenate(
            [
                jnp.dot(normed, weight_part, preferred_element_type=jnp.float32)
                for weight_part in weight_list
            ],
            axis=1,
        ).astype(jnp.bfloat16),
        KV,
        0,
    )
    own_squares = lax.dynamic_slice_in_dim(squares, lax.axis_index(KV) * own_rows, own_rows, 0)
    projected = projected * lax.rsqrt(own_squares / D + epsilon)[:, None]
    pre_query, pre_forget, pre_value, pre_gate_out = jnp.split(projected, 4, axis=1)
    local_heads = past_state.shape[1]
    head_width = past_state.shape[2]
    head_shape = (own_rows, local_heads, head_width)
    floors = forget_floor.reshape(local_heads, head_width)
    forget_heads = pre_forget.reshape(head_shape)
    forget = floors + (1.0 - floors) * jax.nn.sigmoid(forget_heads)
    written = (1.0 - floors) * jax.nn.sigmoid(-forget_heads)
    query_act = jax.nn.silu(pre_query.reshape(head_shape))
    value_act = pre_value.reshape(head_shape)
    new_state = (
        forget[:, :, :, None] * past_state + written[:, :, :, None] * value_act[:, :, None, :]
    )
    readout = jnp.einsum("bhkv,bhk->bhv", new_state, query_act, precision=lax.Precision.HIGHEST)
    readout = (
        readout
        * lax.rsqrt(jnp.mean(readout * readout, axis=2, keepdims=True) + epsilon)
        * head_gain
    )
    mixed_in = (
        readout.reshape(own_rows, local_heads * head_width) * jax.nn.silu(pre_gate_out)
    ).astype(jnp.bfloat16)
    partials = jnp.dot(
        collect(mixed_in, KV, 0), proj_out, preferred_element_type=jnp.float32
    ).astype(jnp.bfloat16)
    mixed_sum = sum_at_owner(partials, TP, 1)
    second = (after_first.astype(jnp.float32) + mixed_sum).astype(jnp.bfloat16)
    hidden_two = half_inputs(second, post_gain, post_gate, post_up)
    result = (second.astype(jnp.float32) + 0.5 * down_sum(hidden_two, post_down)).astype(
        jnp.bfloat16
    )
    return (result, new_state)


def solution(mesh):
    torus = Mesh(mesh.devices.reshape(4, 4, 4, 2), ("kv_0", "kv_1", "tp_0", "tp_1"))
    return jax.shard_map(
        per_device,
        mesh=torus,
        in_specs=(
            P(None, KV_TP),
            P(KV, TP, None, None),
            P(),
            P(None, KV_TP),
            P(None, KV_TP),
            P(KV_TP, None),
            P(),
            P(KV, TP),
            P(KV, TP),
            P(KV, TP),
            P(KV, TP),
            P(TP),
            P(),
            P(TP, KV),
            P(),
            P(None, KV_TP),
            P(None, KV_TP),
            P(KV_TP, None),
        ),
        out_specs=(P(None, KV_TP), P(KV, TP, None, None)),
        check_vma=False,
    )
```

profile of v0, /device:TPU:0, one launch (start us, length us, event | category | flops | bytes accessed | tf_op | source)
XLA Modules:
  0.0 312.5 jit_solution(2136292234413515563)
XLA Ops:
  1.7 41.3 %all_to_all.60 = bf16[64,512,32]{1,2,0:T(8,128)(2,1)S(1)} all-to-all(bf16[64,512,32]{1,2,0:T(8,128)(2,1)S(1)} %broadcast_in_dim.12), channel_id=1, replica_groups=mesh['kv_0'=4,'kv_1'=4,'tp_0'=4,'tp_1'=2] {'kv_0','kv_1','tp_0'}, dimensions={0} | all-to-all | bytes 4194304 | tf_op jit(solution)/shard_map/all_to_all | solution.py:20
  43.6 7.1 %all_to_all.61 = bf16[2,64,512,32]{2,3,1,0:T(8,128)(2,1)S(1)} all-to-all(bf16[2,64,512,32]{2,3,1,0:T(8,128)(2,1)S(1)} %broadcast_in_dim.13), channel_id=1, replica_groups=mesh['kv_0'=4,'kv_1'=4,'tp_0'=4,'tp_1'=2] {'tp_1'}, dimensions={0} | all-to-all | bytes 8388608 | tf_op jit(solution)/shard_map/all_to_all | solution.py:20
  57.3 6.2 %convolution_convert_fusion.1 = bf16[512,4096]{1,0:T(8,128)(2,1)} fusion(bf16[88,4096]{1,0:T(8,128)(2,1)S(1)} %copy-done, bf16[512,4096]{0,1:T(8,128)(2,1)} %copy-done.2, bf16[4096,88]{0,1:T(8,128)(2,1)S(1)} %copy-done.7, f32[512,88]{0,1:T(8,128)S(1)} %convolution_multiply_fusion.3, f32[512]{0:T(512)S(1)} %add_rsqrt_fusion.2), kind=kOutput, calls=%fused_computation.7 | convolution fusion | flops 740610048 | bytes 10012672 | tf_op jit(solution)/shard_map/dot_general | solution.py:80
  63.5 6.4 %copy.27 = bf16[512,4096]{0,1:T(8,128)(2,1)} copy(bf16[512,4096]{1,0:T(8,128)(2,1)} %convolution_convert_fusion.1) | data formatting | bytes 8388608 | tf_op jit(solution)/shard_map/convert_element_type | solution.py:80
  72.6 8.2 %all_to_all.62 = bf16[2,64,512,32]{2,3,1,0:T(8,128)(2,1)} all-to-all(bf16[2,64,512,32]{2,3,1,0:T(8,128)(2,1)S(1)} %copy.28), channel_id=1, replica_groups=mesh['kv_0'=4,'kv_1'=4,'tp_0'=4,'tp_1'=2] {'tp_1'}, dimensions={0} | all-to-all | bytes 8388608 | tf_op jit(solution)/shard_map/all_to_all | solution.py:43
  80.7 3.4 %reduce_sum.97 = bf16[64,512,32]{1,2,0:T(8,128)(2,1)S(1)} reduce(bf16[2,64,512,32]{2,3,1,0:T(8,128)(2,1)} %all_to_all.62, bf16[]{:T(256)} %constant.19.clone.1), dimensions={0}, to_apply=%region_1.2 | reduce | flops 1048576 | bytes 6291458 | tf_op jit(solution)/shard_map/reduce_sum | solution.py:44
  84.2 36.0 %all_to_all.63 = bf16[64,512,32]{1,2,0:T(8,128)(2,1)S(1)} all-to-all(bf16[64,512,32]{1,2,0:T(8,128)(2,1)S(1)} %reduce_sum.97), channel_id=1, replica_groups=mesh['kv_0'=4,'kv_1'=4,'tp_0'=4,'tp_1'=2] {'kv_0','kv_1','tp_0'}, dimensions={0} | all-to-all | bytes 4194304 | tf_op jit(solution)/shard_map/all_to_all | solution.py:51
  121.3 3.4 %all-to-all-start.4 = ((bf16[8,512,32]{1,2,0:T(8,128)(2,1)}), bf16[8,512,32]{1,2,0:T(8,128)(2,1)S(1)}, u32[]{:S(2)}, u32[]{:S(2)}) async-start(bf16[8,512,32]{1,2,0:T(8,128)(2,1)} %broadcast_in_dim.14), calls=%async_computation.4 | async-start | bytes 524288 | tf_op jit(solution)/shard_map/all_to_all | solution.py:20
  125.5 6.7 %all-to-all-done.4 = bf16[8,512,32]{1,2,0:T(8,128)(2,1)S(1)} async-done(((bf16[8,512,32]{1,2,0:T(8,128)(2,1)}), bf16[8,512,32]{1,2,0:T(8,128)(2,1)S(1)}, u32[]{:S(2)}, u32[]{:S(2)}) %all-to-all-start.4) | async-done | bytes 262176 | tf_op jit(solution)/shard_map/all_to_all | solution.py:20
  137.7 3.8 %all-to-all-start.5 = ((bf16[16,32,1024]{2,1,0:T(8,128)(2,1)}), bf16[16,32,1024]{2,1,0:T(8,128)(2,1)S(1)}, u32[]{:S(2)}, u32[]{:S(2)}) async-start(bf16[16,32,1024]{2,1,0:T(8,128)(2,1)} %pad_maximum_fusion), calls=%async_computation.5 | async-start | bytes 2097152 | tf_op jit(solution)/shard_map/all_to_all | solution.py:43
  141.6 15.7 %psum.14 = f32[512]{0:T(512)S(1)} all-reduce(f32[512]{0:T(512)S(1)} %fusion.6), channel_id=1, replica_groups=mesh['kv_0'=4,'kv_1'=4,'tp_0'=4,'tp_1'=2] {'kv_0'}, use_global_device_ids=true, to_apply=%region_5.6 | all-reduce | flops 512 | bytes 4096 | tf_op jit(solution)/shard_map/psum | solution.py:63
  157.3 11.7 %psum.15 = f32[512]{0:T(512)S(1)} all-reduce(f32[512]{0:T(512)S(1)} %psum.14), channel_id=1, replica_groups=mesh['kv_0'=4,'kv_1'=4,'tp_0'=4,'tp_1'=2] {'kv_1'}, use_global_device_ids=true, to_apply=%region_6.7 | all-reduce | flops 512 | bytes 4096 | tf_op jit(solution)/shard_map/psum | solution.py:63
  169.7 4.4 %multiply_add_fusion = f32[32,2,128,128]{3,2,1,0:T(8,128)S(1)} fusion(f32[32,2,128,128]{3,2,1,0:T(8,128)} %param.19, f32[32,2,128]{2,1,0:T(2,128)S(1)} %mul.208, f32[32,2,128]{2,1,0:T(2,128)S(1)} %bitcast.97, f32[32,2,128]{2,1,0:T(2,128)S(1)} %bitcast.96), kind=kLoop, calls=%fused_computation.11 | loop fusion | flops 3145728 | bytes 8486912 | tf_op jit(solution)/shard_map/add | solution.py:144
  174.1 3.6 %fusion.29 = f32[32,2,1,128]{3,2,1,0:T(1,128)S(1)} fusion(f32[32,2,128,128]{3,2,1,0:T(8,128)S(1)} %multiply_add_fusion, f32[32,2,128,1]{2,3,1,0:T(1,128)S(1)} %bitcast.98), kind=kOutput, calls=%fused_computation.72 | convolution fusion | flops 12582912 | bytes 4259840 | tf_op jit(solution)/shard_map/bhkv,bhk->bhv/dot_general | solution.py:146
  178.0 11.3 %all_to_all.64 = bf16[16,32,256]{2,1,0:T(8,128)(2,1)S(1)} all-to-all(bf16[16,32,256]{2,1,0:T(8,128)(2,1)S(1)} %broadcast_in_dim.15), channel_id=1, replica_groups=mesh['kv_0'=4,'kv_1'=4,'tp_0'=4,'tp_1'=2] {'kv_0','kv_1'}, dimensions={0} | all-to-all | bytes 524288 | tf_op jit(solution)/shard_map/all_to_all | solution.py:20
  189.6 9.9 %all_to_all.65 = bf16[8,512,32]{1,2,0:T(8,128)(2,1)S(1)} all-to-all(bf16[8,512,32]{1,2,0:T(8,128)(2,1)S(1)} %bitcast.93), channel_id=1, replica_groups=mesh['kv_0'=4,'kv_1'=4,'tp_0'=4,'tp_1'=2] {'tp_0','tp_1'}, dimensions={0} | all-to-all | bytes 524288 | tf_op jit(solution)/shard_map/all_to_all | solution.py:43
  199.8 34.0 %all_to_all.66 = bf16[64,512,32]{1,2,0:T(8,128)(2,1)S(1)} all-to-all(bf16[64,512,32]{1,2,0:T(8,128)(2,1)S(1)} %broadcast_in_dim.16), channel_id=1, replica_groups=mesh['kv_0'=4,'kv_1'=4,'tp_0'=4,'tp_1'=2] {'kv_0','kv_1','tp_0'}, dimensions={0} | all-to-all | bytes 4194304 | tf_op jit(solution)/shard_map/all_to_all | solution.py:20
  234.4 7.1 %all_to_all.67 = bf16[2,64,512,32]{2,3,1,0:T(8,128)(2,1)S(1)} all-to-all(bf16[2,64,512,32]{2,3,1,0:T(8,128)(2,1)S(1)} %broadcast_in_dim.17), channel_id=1, replica_groups=mesh['kv_0'=4,'kv_1'=4,'tp_0'=4,'tp_1'=2] {'tp_1'}, dimensions={0} | all-to-all | bytes 8388608 | tf_op jit(solution)/shard_map/all_to_all | solution.py:20
  248.3 6.2 %convolution_convert_fusion = bf16[512,4096]{1,0:T(8,128)(2,1)} fusion(bf16[88,4096]{1,0:T(8,128)(2,1)S(1)} %copy-done.8, bf16[512,4096]{0,1:T(8,128)(2,1)} %copy-done.3, bf16[4096,88]{0,1:T(8,128)(2,1)S(1)} %copy-done.9, f32[512,88]{0,1:T(8,128)S(1)} %convolution_multiply_fusion.1, f32[512]{0:T(512)S(1)} %add_rsqrt_fusion.1), kind=kOutput, calls=%fused_computation.6 | convolution fusion | flops 740610048 | bytes 10012672 | tf_op jit(solution)/shard_map/dot_general | solution.py:80
  254.5 6.5 %copy.32 = bf16[512,4096]{0,1:T(8,128)(2,1)} copy(bf16[512,4096]{1,0:T(8,128)(2,1)} %convolution_convert_fusion) | data formatting | bytes 8388608 | tf_op jit(solution)/shard_map/convert_element_type | solution.py:80
  261.1 2.7 copy.33
  263.7 8.2 %all_to_all.68 = bf16[2,64,512,32]{2,3,1,0:T(8,128)(2,1)} all-to-all(bf16[2,64,512,32]{2,3,1,0:T(8,128)(2,1)S(1)} %copy.33), channel_id=1, replica_groups=mesh['kv_0'=4,'kv_1'=4,'tp_0'=4,'tp_1'=2] {'tp_1'}, dimensions={0} | all-to-all | bytes 8388608 | tf_op jit(solution)/shard_map/all_to_all | solution.py:43
  271.9 3.5 %reduce_sum.104 = bf16[64,512,32]{1,2,0:T(8,128)(2,1)S(1)} reduce(bf16[2,64,512,32]{2,3,1,0:T(8,128)(2,1)} %all_to_all.68, bf16[]{:T(256)} %constant.19.clone.1), dimensions={0}, to_apply=%region_10.11 | reduce | flops 1048576 | bytes 6291458 | tf_op jit(solution)/shard_map/reduce_sum | solution.py:44
  275.4 36.1 %all_to_all.69 = bf16[64,512,32]{1,2,0:T(8,128)(2,1)S(1)} all-to-all(bf16[64,512,32]{1,2,0:T(8,128)(2,1)S(1)} %reduce_sum.104), channel_id=1, replica_groups=mesh['kv_0'=4,'kv_1'=4,'tp_0'=4,'tp_1'=2] {'kv_0','kv_1','tp_0'}, dimensions={0} | all-to-all | bytes 4194304 | tf_op jit(solution)/shard_map/all_to_all | solution.py:51
  (89 shorter events, 27.9 us)
Async XLA Ops:
  0.6 56.4 %copy-start = (bf16[88,4096]{1,0:T(8,128)(2,1)S(1)}, bf16[88,4096]{1,0:T(8,128)(2,1)}, u32[]{:S(2)}) copy-start(bf16[88,4096]{1,0:T(8,128)(2,1)} %param.23) | copy-start | bytes 2162692
  51.6 1.2 copy-start.14
  52.9 3.3 %copy-start.5 = (bf16[4096,88]{0,1:T(8,128)(2,1)S(1)}, bf16[4096,88]{0,1:T(8,128)(2,1)}, u32[]{:S(2)}) copy-start(bf16[4096,88]{0,1:T(8,128)(2,1)} %param.21) | copy-start | bytes 2162692
  54.2 2.0 copy-start.2
  56.2 1.1 copy-start.7
  84.2 36.4 %copy-start.10 = (bf16[512,32]{0,1:T(8,128)(2,1)S(1)}, bf16[512,32]{0,1:T(8,128)(2,1)}, u32[]{:S(2)}) copy-start(bf16[512,32]{0,1:T(8,128)(2,1)} %param.18) | copy-start | bytes 98308
  120.5 13.3 %copy-start.11 = (bf16[256,256]{1,0:T(8,128)(2,1)S(1)}, bf16[256,256]{1,0:T(8,128)(2,1)}, u32[]{:S(2)}) copy-start(bf16[256,256]{1,0:T(8,128)(2,1)} %param.28) | copy-start | bytes 393220
  120.6 13.5 %copy-start.12 = (bf16[256,256]{1,0:T(8,128)(2,1)S(1)}, bf16[256,256]{1,0:T(8,128)(2,1)}, u32[]{:S(2)}) copy-start(bf16[256,256]{1,0:T(8,128)(2,1)} %param.27) | copy-start | bytes 393220
  121.3 10.9 %all-to-all-start.4 = ((bf16[8,512,32]{1,2,0:T(8,128)(2,1)}), bf16[8,512,32]{1,2,0:T(8,128)(2,1)S(1)}, u32[]{:S(2)}, u32[]{:S(2)}) async-start(bf16[8,512,32]{1,2,0:T(8,128)(2,1)} %broadcast_in_dim.14), calls=%async_computation.4 | async-start | bytes 524288 | tf_op jit(solution)/shard_map/all_to_all | solution.py:20
  133.8 7.8 %copy-start.16 = (f32[256]{0:T(256)S(1)}, f32[256]{0:T(256)}, u32[]{:S(2)}) copy-start(f32[256]{0:T(256)} %param.29) | copy-start | bytes 3076
  137.7 31.5 %all-to-all-start.5 = ((bf16[16,32,1024]{2,1,0:T(8,128)(2,1)}), bf16[16,32,1024]{2,1,0:T(8,128)(2,1)S(1)}, u32[]{:S(2)}, u32[]{:S(2)}) async-start(bf16[16,32,1024]{2,1,0:T(8,128)(2,1)} %pad_maximum_fusion), calls=%async_computation.5 | async-start | bytes 2097152 | tf_op jit(solution)/shard_map/all_to_all | solution.py:43
  174.1 25.8 %copy-start.4 = (f32[32,2,128,128]{3,2,1,0:T(8,128)}, f32[32,2,128,128]{3,2,1,0:T(8,128)S(1)}, u32[]{:S(2)}) copy-start(f32[32,2,128,128]{3,2,1,0:T(8,128)S(1)} %multiply_add_fusion) | copy-start | bytes 12582916
  174.1 3.8 %copy-start.17 = (f32[128]{0:T(128)S(1)}, f32[128]{0:T(128)}, u32[]{:S(2)}) copy-start(f32[128]{0:T(128)} %param.30) | copy-start | bytes 1540
  174.1 15.3 %copy-start.13 = (bf16[256,256]{1,0:T(8,128)(2,1)S(1)}, bf16[256,256]{1,0:T(8,128)(2,1)}, u32[]{:S(2)}) copy-start(bf16[256,256]{1,0:T(8,128)(2,1)} %param.31) | copy-start | bytes 393220
  242.5 1.2 copy-start.15
  243.7 3.3 %copy-start.6 = (bf16[4096,88]{0,1:T(8,128)(2,1)S(1)}, bf16[4096,88]{0,1:T(8,128)(2,1)}, u32[]{:S(2)}) copy-start(bf16[4096,88]{0,1:T(8,128)(2,1)} %param.33) | copy-start | bytes 2162692
  245.0 2.0 copy-start.3
  247.0 1.1 copy-start.8
  247.0 1.3 copy-start.9
  271.9 40.6 %copy-start.1 = (bf16[88,4096]{1,0:T(8,128)(2,1)S(1)}, bf16[88,4096]{1,0:T(8,128)(2,1)}, u32[]{:S(2)}) copy-start(bf16[88,4096]{1,0:T(8,128)(2,1)} %param.23) | copy-start | bytes 2162692
where the time goes:
time: 314 us; the launch traced here: 312 us
  blocking collectives  227 us (72%)
  local copies, waits for them, and re-layouts  28.6 us (9%)
  other arithmetic  21.5 us (7%)
  matrix products  20.7 us (7%)
  starting transfers between devices  7.25 us (2%)
  waiting for transfers between devices  6.66 us (2%)
    all_to_all x5, blocking collectives, copy_for_each(): return lax.all_to_all(copies, axis, split_axis=0, concat_axis=0, tiled=True)  101 us
    all_to_all x2, blocking collectives, summed_rows(): lax.all_to_all(nearer.astype(jnp.bfloat16), far, split_axis=0, concat_axi...  72.2 us
    psum x2, blocking collectives, over_axes(): return functools.reduce(lax.psum, axes, value)  27.4 us
    all_to_all x3, blocking collectives, sum_at_owner(): lax.all_to_all(split_up(value, dim, devices), axis, 0, 0, tiled=True)  26.3 us
    convert_element_type x2, local copies, waits for them, and re-layouts, down_sum(): jnp.dot(hidden, w_down, preferred_element_type=jnp.float32)  12.9 us
    dot_general x2, matrix products, down_sum(): jnp.dot(hidden, w_down, preferred_element_type=jnp.float32)  12.4 us
    reduce_sum x4, other arithmetic, sum_at_owner(): return jnp.sum(pieces.astype(jnp.float32), axis=0)  7.09 us
    all_to_all x1, waiting for transfers between devices, copy_for_each(): return lax.all_to_all(copies, axis, split_axis=0, concat_axis=0, tiled=True)  6.66 us
  transfers between devices with their start and end apart: 2, of which 1 were waited for; matrix products, arithmetic and copies ran while one was open for 0% of the time, Pallas kernels for 0%

commit v1 on v0

v1 whole, which is shorter than its diff:
```python
import jax
import jax.numpy as jnp
from jax import lax
from jax.sharding import Mesh
from jax.sharding import PartitionSpec as P

D = 4096
ALL = ("z", "y", "x", "c")
KV = ("z", "y")
TP = ("x", "c")
SAME_CORE = ("z", "y", "x")
epsilon = 1e-06
f32 = jnp.float32
bf16 = jnp.bfloat16


def copy_for_each(value, axes):
    copies = jnp.broadcast_to(value, (lax.axis_size(axes), *value.shape))
    return lax.all_to_all(copies, axes, split_axis=0, concat_axis=0, tiled=True)


def exchange(pieces, axes):
    return lax.all_to_all(pieces, axes, split_axis=0, concat_axis=0, tiled=True)


def other_core(value):
    return lax.ppermute(value, "c", [(0, 1), (1, 0)])


def dot_t(left, right):
    return lax.dot_general(left, right, (((1,), (0,)), ((), ())), preferred_element_type=f32)


def half_step(own, gain, gate, up, down, gate_far, up_far, down_far):
    core = lax.axis_index("c")
    chips = lax.axis_size(SAME_CORE)
    width, rows = own.shape
    units = gate.shape[0]
    pieces = copy_for_each(own, SAME_CORE).astype(f32)
    squares = jnp.sum(pieces * pieces, axis=(0, 1))
    parity = lax.broadcasted_iota(jnp.int32, (1, 2, 1, 1), 1)
    gains = gain.reshape(chips, 2, width, 1)
    normed = jnp.where(parity == core, pieces[:, None] * gains, 0.0).astype(bf16)
    normed = normed.reshape(chips * 2 * width, rows)
    parts = [dot_t(w, normed) for w in (gate, up, gate_far, up_far)]
    sent = jnp.concatenate([*parts, jnp.broadcast_to(squares, (8, rows))], axis=0)
    got = other_core(sent)
    g_own = parts[0] + got[2 * units : 3 * units]
    u_own = parts[1] + got[3 * units : 4 * units]
    g_far = parts[2] + got[:units]
    u_far = parts[3] + got[units : 2 * units]
    scale = lax.rsqrt((squares + got[4 * units]) / D + epsilon)[None, :]
    hidden = jnp.concatenate(
        [
            (jax.nn.silu(scale * g_own) * (scale * u_own)).astype(bf16),
            (jax.nn.silu(scale * g_far) * (scale * u_far)).astype(bf16),
        ],
        axis=0,
    )
    weights = jnp.concatenate([down, down_far], axis=0)
    out = lax.dot_general(weights, hidden, (((0,), (0,)), ((), ())), preferred_element_type=f32)
    out = out.astype(bf16).reshape(chips, 2, width, rows)
    out = jnp.where(core == 0, out[:, 0], out[:, 1])
    total = jnp.sum(exchange(out, SAME_CORE).astype(f32), axis=0)
    return (own.astype(f32) + 0.5 * total).astype(bf16)


def per_device(
    tokens,
    past_state,
    pre_gain,
    pre_gate,
    pre_up,
    pre_down,
    mix_gain,
    query_weight,
    forget_weight,
    value_weight,
    output_gate_weight,
    forget_floor,
    head_gain,
    proj_out,
    post_gain,
    post_gate,
    post_up,
    post_down,
):
    pre = [pre_gate.T, pre_up.T, pre_down]
    post = [post_gate.T, post_up.T, post_down]
    first = half_step(tokens.T, pre_gain, *pre, *[other_core(w) for w in pre])

    block = copy_for_each(first, TP)
    block = block.reshape(-1, block.shape[2])
    width, rows = block.shape
    own_rows, local_heads, head_width, _ = past_state.shape
    block_float = block.astype(f32)
    gains = lax.dynamic_slice_in_dim(mix_gain, lax.axis_index(KV) * width, width, 0)
    squares = jnp.sum(block_float * block_float, axis=0)
    square_high = squares.astype(bf16)
    square_low = (squares - square_high.astype(f32)).astype(bf16)
    normed = (block_float * gains[:, None]).astype(bf16).T
    weight_list = (query_weight, forget_weight, value_weight, output_gate_weight)
    parts = [jnp.dot(normed, w, preferred_element_type=f32).astype(bf16) for w in weight_list]
    parts += [
        jnp.broadcast_to(square_high[:, None], (rows, 128)),
        jnp.broadcast_to(square_low[:, None], (rows, 128)),
    ]
    sent = jnp.concatenate(parts, axis=1).reshape(-1, own_rows, 4 * width + 256)
    projected = jnp.sum(exchange(sent, KV).astype(f32), axis=0)
    own_squares = projected[:, 4 * width] + projected[:, 4 * width + 128]
    projected = projected[:, : 4 * width] * lax.rsqrt(own_squares / D + epsilon)[:, None]
    pre_query, pre_forget, pre_value, pre_gate_out = jnp.split(projected, 4, axis=1)
    head_shape = (own_rows, local_heads, head_width)
    floors = forget_floor.reshape(local_heads, head_width)
    forget_heads = pre_forget.reshape(head_shape)
    forget = floors + (1.0 - floors) * jax.nn.sigmoid(forget_heads)
    written = (1.0 - floors) * jax.nn.sigmoid(-forget_heads)
    query_act = jax.nn.silu(pre_query.reshape(head_shape))
    value_act = pre_value.reshape(head_shape)
    new_state = (
        forget[:, :, :, None] * past_state + written[:, :, :, None] * value_act[:, :, None, :]
    )
    readout = jnp.einsum("bhkv,bhk->bhv", new_state, query_act, precision=lax.Precision.HIGHEST)
    readout = (
        readout
        * lax.rsqrt(jnp.mean(readout * readout, axis=2, keepdims=True) + epsilon)
        * head_gain
    )
    mixed_in = (
        readout.reshape(own_rows, local_heads * head_width) * jax.nn.silu(pre_gate_out)
    ).astype(bf16)
    gathered = copy_for_each(mixed_in, KV).reshape(rows, local_heads * head_width)
    partials = lax.dot_general(
        proj_out, gathered, (((0,), (1,)), ((), ())), preferred_element_type=f32
    ).astype(bf16)
    mixed_sum = jnp.sum(exchange(partials.reshape(-1, *first.shape), TP).astype(f32), axis=0)
    second = (first.astype(f32) + mixed_sum).astype(bf16)
    result = half_step(second, post_gain, *post, *[other_core(w) for w in post])
    return (result.T, new_state)


def solution(mesh):
    torus = Mesh(mesh.devices.reshape(4, 4, 4, 2), ALL)
    return jax.shard_map(
        per_device,
        mesh=torus,
        in_specs=(
            P(None, ALL),
            P(KV, TP, None, None),
            P(),
            P(None, ALL),
            P(None, ALL),
            P(ALL, None),
            P(),
            P(KV, TP),
            P(KV, TP),
            P(KV, TP),
            P(KV, TP),
            P(TP),
            P(),
            P(TP, KV),
            P(),
            P(None, ALL),
            P(None, ALL),
            P(ALL, None),
        ),
        out_specs=(P(None, ALL), P(KV, TP, None, None)),
        check_vma=False,
    )
```

time: 314 us -> 258 us (0.82)
  blocking collectives: 227 us -> 94.1 us
  waiting for transfers between devices: 6.66 us -> 91 us
  local copies, waits for them, and re-layouts: 28.6 us -> 9.96 us
  starting transfers between devices: 7.25 us -> 25.8 us
  other arithmetic: 21.5 us -> 12.5 us
    all_to_all x10 -> x4, blocking collectives: 199 us -> 94.1 us  [the longest x3 82.1 us: exchange(): return lax.all_to_all(pieces, axes, split_axis=0, concat_axis=0, tiled=True)]
    all_to_all x2 -> x4, waiting for transfers between devices: 6.66 us -> 85.6 us  [the longest x3 65.1 us: copy_for_each(): return lax.all_to_all(copies, axes, split_axis=0, concat_axis=0, tiled=True)]
    psum x2 -> x0, blocking collectives: 27.4 us -> none  [over_axes(): return functools.reduce(lax.psum, axes, value)]
    all_to_all x2 -> x4, starting transfers between devices: 7.25 us -> 23.5 us  [the longest x3 19.6 us: copy_for_each(): return lax.all_to_all(copies, axes, split_axis=0, concat_axis=0, tiled=True)]
    convert_element_type x4 -> x0, local copies, waits for them, and re-layouts: 14.5 us -> none  [the longest x2 12.9 us: down_sum(): jnp.dot(hidden, w_down, preferred_element_type=jnp.float32)]
    reduce_sum x9 -> x7, other arithmetic: 9.76 us -> 2.03 us  [the longest x2 1.07 us: half_step(): squares = jnp.sum(pieces * pieces, axis=(0, 1))]
    ppermute x0 -> x8, waiting for transfers between devices: none -> 5.4 us  [other_core(): return lax.ppermute(value, 'c', [(0, 1), (1, 0)])]
    transpose x2 -> x0, local copies, waits for them, and re-layouts: 5.32 us -> none  [split_up(): return jnp.moveaxis(pieces, dim, 0)]
  transfers between devices with their start and end apart: 2 -> 12, of which waited for: 1 -> 8; matrix products, arithmetic and copies ran while one was open for 0% -> 6% of each run, Pallas kernels for 0% -> 0%
where the time goes in v1:
time: 258 us; the launch traced here: 257 us
  blocking collectives  94.1 us (36%)
  waiting for transfers between devices  91 us (35%)
  starting transfers between devices  25.8 us (10%)
  matrix products  22.6 us (9%)
  other arithmetic  12.5 us (5%)
  local copies, waits for them, and re-layouts  9.96 us (4%)
    all_to_all x3, blocking collectives, exchange(): return lax.all_to_all(pieces, axes, split_axis=0, concat_axis=0, tiled=True)  82.1 us
    all_to_all x3, waiting for transfers between devices, copy_for_each(): return lax.all_to_all(copies, axes, split_axis=0, concat_axis=0, tiled=True)  65.1 us
    all_to_all x1, waiting for transfers between devices, exchange(): return lax.all_to_all(pieces, axes, split_axis=0, concat_axis=0, tiled=True)  20.5 us
    all_to_all x3, starting transfers between devices, copy_for_each(): return lax.all_to_all(copies, axes, split_axis=0, concat_axis=0, tiled=True)  19.6 us
    dot_general x8, matrix products, dot_t(): lax.dot_general(left, right, (((1,), (0,)), ((), ())), preferred_element_...  13.9 us
    all_to_all x1, blocking collectives, copy_for_each(): return lax.all_to_all(copies, axes, split_axis=0, concat_axis=0, tiled=True)  12 us
    ppermute x8, waiting for transfers between devices, other_core(): return lax.ppermute(value, 'c', [(0, 1), (1, 0)])  5.4 us
  transfers between devices with their start and end apart: 12, of which 8 were waited for; matrix products, arithmetic and copies ran while one was open for 6% of the time, Pallas kernels for 0%

profile of v1, /device:TPU:0, one launch (start us, length us, event | category | flops | bytes accessed | tf_op | source)
XLA Modules:
  0.0 257.2 jit_solution(12621663074490422570)
XLA Ops:
  0.7 2.4 broadcast_in_dim.62
  3.1 11.5 %all-to-all-start = ((bf16[64,32,512]{2,1,0:T(8,128)(2,1)}), bf16[64,32,512]{2,1,0:T(8,128)(2,1)S(1)}, u32[]{:S(2)}, u32[]{:S(2)}) async-start(bf16[64,32,512]{2,1,0:T(8,128)(2,1)} %broadcast_in_dim.62), calls=%async_computation | async-start | bytes 4194304 | tf_op jit(solution)/shard_map/all_to_all | solution.py:19
  15.4 29.1 %all-to-all-done = bf16[64,32,512]{2,1,0:T(8,128)(2,1)S(1)} async-done(((bf16[64,32,512]{2,1,0:T(8,128)(2,1)}), bf16[64,32,512]{2,1,0:T(8,128)(2,1)S(1)}, u32[]{:S(2)}, u32[]{:S(2)}) %all-to-all-start) | async-done | bytes 2097184 | tf_op jit(solution)/shard_map/all_to_all | solution.py:19
  50.1 2.7 %constant_dynamic-update-slice_fusion.2 = (f32[360,512]{1,0:T(8,128)}, f32[88,512]{1,0:T(8,128)S(1)}) fusion(f32[360,512]{1,0:T(8,128)} %get-tuple-element.16, bf16[4096,512]{1,0:T(8,128)(2,1)S(1)} %fusion.3, bf16[88,4096]{1,0:T(8,128)(2,1)} %collective-permute-done.1), kind=kOutput, calls=%fused_computation.88 | convolution fusion | flops 369098752 | bytes 5275648 | tf_op jit(solution)/shard_map/dot_general | solution.py:31
  52.8 2.6 %constant_dynamic-update-slice_fusion.1 = (f32[360,512]{1,0:T(8,128)}, f32[88,512]{1,0:T(8,128)S(1)}) fusion(f32[360,512]{1,0:T(8,128)} %get-tuple-element.18, bf16[4096,512]{1,0:T(8,128)(2,1)S(1)} %fusion.3, bf16[88,4096]{1,0:T(8,128)(2,1)} %collective-permute-done.2), kind=kOutput, calls=%fused_computation.87 | convolution fusion | flops 369098752 | bytes 5275648 | tf_op jit(solution)/shard_map/dot_general | solution.py:31
  56.6 1.9 collective-permute-done.3
  59.6 2.4 convolution_convert_fusion.1
  62.3 36.2 %all_to_all.40 = bf16[64,32,512]{2,1,0:T(8,128)(2,1)S(1)} all-to-all(bf16[64,32,512]{2,1,0:T(8,128)(2,1)S(1)} %fusion.5), channel_id=1, replica_groups=mesh['z'=4,'y'=4,'x'=4,'c'=2] {'z','y','x'}, dimensions={0} | all-to-all | bytes 4194304 | tf_op jit(solution)/shard_map/all_to_all | solution.py:23
  99.6 3.4 %all-to-all-start.2 = ((bf16[8,32,512]{2,1,0:T(8,128)(2,1)}), bf16[8,32,512]{2,1,0:T(8,128)(2,1)S(1)}, u32[]{:S(2)}, u32[]{:S(2)}) async-start(bf16[8,32,512]{2,1,0:T(8,128)(2,1)} %broadcast_in_dim.68), calls=%async_computation.2 | async-start | bytes 524288 | tf_op jit(solution)/shard_map/all_to_all | solution.py:19
  103.8 6.7 %all-to-all-done.2 = bf16[8,32,512]{2,1,0:T(8,128)(2,1)S(1)} async-done(((bf16[8,32,512]{2,1,0:T(8,128)(2,1)}), bf16[8,32,512]{2,1,0:T(8,128)(2,1)S(1)}, u32[]{:S(2)}, u32[]{:S(2)}) %all-to-all-start.2) | async-done | bytes 262176 | tf_op jit(solution)/shard_map/all_to_all | solution.py:19
  113.3 3.9 %all-to-all-start.3 = ((bf16[16,32,1280]{2,1,0:T(8,128)(2,1)}), bf16[16,32,1280]{2,1,0:T(8,128)(2,1)S(1)}, u32[]{:S(2)}, u32[]{:S(2)}) async-start(bf16[16,32,1280]{2,1,0:T(8,128)(2,1)} %bitcast.15), calls=%async_computation.3 | async-start | bytes 2621440 | tf_op jit(solution)/shard_map/all_to_all | solution.py:23
  117.2 20.5 %all-to-all-done.3 = bf16[16,32,1280]{2,1,0:T(8,128)(2,1)S(1)} async-done(((bf16[16,32,1280]{2,1,0:T(8,128)(2,1)}), bf16[16,32,1280]{2,1,0:T(8,128)(2,1)S(1)}, u32[]{:S(2)}, u32[]{:S(2)}) %all-to-all-start.3) | async-done | bytes 1310752 | tf_op jit(solution)/shard_map/all_to_all | solution.py:23
  138.3 4.4 %multiply_add_fusion = f32[32,2,128,128]{3,2,1,0:T(8,128)S(1)} fusion(f32[32,2,128,128]{3,2,1,0:T(8,128)} %param.19, f32[32,2,128]{2,1,0:T(2,128)S(1)} %mul.267, f32[32,2,128]{2,1,0:T(2,128)S(1)} %bitcast.129, f32[32,2,128]{2,1,0:T(2,128)S(1)} %bitcast.128), kind=kLoop, calls=%fused_computation.10 | loop fusion | flops 3145728 | bytes 8486912 | tf_op jit(solution)/shard_map/add | solution.py:121
  142.7 2.0 copy-done.2
  144.7 3.6 %fusion.52 = f32[32,2,1,128]{3,2,1,0:T(1,128)S(1)} fusion(f32[32,2,128,128]{3,2,1,0:T(8,128)S(1)} %multiply_add_fusion, f32[32,2,128,1]{2,3,1,0:T(1,128)S(1)} %bitcast.130), kind=kOutput, calls=%fused_computation.123 | convolution fusion | flops 12582912 | bytes 4259840 | tf_op jit(solution)/shard_map/bhkv,bhk->bhv/dot_general | solution.py:123
  148.7 12.0 %all_to_all.41 = bf16[16,32,256]{2,1,0:T(8,128)(2,1)S(1)} all-to-all(bf16[16,32,256]{2,1,0:T(8,128)(2,1)S(1)} %broadcast_in_dim.71), channel_id=1, replica_groups=mesh['z'=4,'y'=4,'x'=4,'c'=2] {'z','y'}, dimensions={0} | all-to-all | bytes 524288 | tf_op jit(solution)/shard_map/all_to_all | solution.py:19
  161.0 9.9 %all_to_all.42 = bf16[8,32,512]{2,1,0:T(8,128)(2,1)S(1)} all-to-all(bf16[8,32,512]{2,1,0:T(8,128)(2,1)S(1)} %bitcast.120), channel_id=1, replica_groups=mesh['z'=4,'y'=4,'x'=4,'c'=2] {'x','c'}, dimensions={0} | all-to-all | bytes 524288 | tf_op jit(solution)/shard_map/all_to_all | solution.py:23
  170.9 1.6 broadcast_in_dim.72
  172.5 4.7 %all-to-all-start.6 = ((bf16[64,32,512]{2,1,0:T(8,128)(2,1)}), bf16[64,32,512]{2,1,0:T(8,128)(2,1)S(1)}, u32[]{:S(2)}, u32[]{:S(2)}) async-start(bf16[64,32,512]{2,1,0:T(8,128)(2,1)} %broadcast_in_dim.72), calls=%async_computation.6 | async-start | bytes 4194304 | tf_op jit(solution)/shard_map/all_to_all | solution.py:19
  177.8 29.3 %all-to-all-done.6 = bf16[64,32,512]{2,1,0:T(8,128)(2,1)S(1)} async-done(((bf16[64,32,512]{2,1,0:T(8,128)(2,1)}), bf16[64,32,512]{2,1,0:T(8,128)(2,1)S(1)}, u32[]{:S(2)}, u32[]{:S(2)}) %all-to-all-start.6) | async-done | bytes 2097184 | tf_op jit(solution)/shard_map/all_to_all | solution.py:19
  211.3 2.0 constant_dynamic-update-slice_fusion.7
  213.4 1.9 constant_dynamic-update-slice_fusion.6
  215.9 1.7 collective-permute-done.7
  220.2 36.0 %all_to_all.43 = bf16[64,32,512]{2,1,0:T(8,128)(2,1)S(1)} all-to-all(bf16[64,32,512]{2,1,0:T(8,128)(2,1)S(1)} %fusion.4), channel_id=1, replica_groups=mesh['z'=4,'y'=4,'x'=4,'c'=2] {'z','y','x'}, dimensions={0} | all-to-all | bytes 4194304 | tf_op jit(solution)/shard_map/all_to_all | solution.py:23
  (108 shorter events, 23.5 us)
Async XLA Ops:
  0.6 110.0 %copy-start = (bf16[256,256]{1,0:T(8,128)(2,1)S(1)}, bf16[256,256]{1,0:T(8,128)(2,1)}, u32[]{:S(2)}) copy-start(bf16[256,256]{1,0:T(8,128)(2,1)} %param.25) | copy-start | bytes 393220
  0.6 14.0 %copy-start.3 = (bf16[4096,88]{0,1:T(8,128)(2,1)S(1)}, bf16[4096,88]{0,1:T(8,128)(2,1)}, u32[]{:S(2)}) copy-start(bf16[4096,88]{0,1:T(8,128)(2,1)} %param.21) | copy-start | bytes 2162692
  3.1 41.5 %all-to-all-start = ((bf16[64,32,512]{2,1,0:T(8,128)(2,1)}), bf16[64,32,512]{2,1,0:T(8,128)(2,1)S(1)}, u32[]{:S(2)}, u32[]{:S(2)}) async-start(bf16[64,32,512]{2,1,0:T(8,128)(2,1)} %broadcast_in_dim.62), calls=%async_computation | async-start | bytes 4194304 | tf_op jit(solution)/shard_map/all_to_all | solution.py:19
  14.6 30.6 %copy-start.12 = (f32[4096]{0:T(1024)S(1)}, f32[4096]{0:T(1024)}, u32[]{:S(2)}) copy-start(f32[4096]{0:T(1024)} %param.20) | copy-start | bytes 49156
  14.6 35.5 %collective-permute-start.1 = (bf16[88,4096]{1,0:T(8,128)(2,1)S(1)}, bf16[88,4096]{1,0:T(8,128)(2,1)}, u32[]{:S(2)}, u32[]{:S(2)}) collective-permute-start(bf16[88,4096]{1,0:T(8,128)(2,1)S(1)} %bitcast.121), channel_id=1, source_target_pairs={{0,1},{1,0},{2,3},{3,2},{4,5},{5,4},{6,7},{7,6},{8,9},{9,8},{10,11... | collective-permute-start | bytes 2162696 | tf_op jit(solution)/shard_map/ppermute | solution.py:27
  14.7 38.1 %collective-permute-start.2 = (bf16[88,4096]{1,0:T(8,128)(2,1)}, bf16[88,4096]{1,0:T(8,128)(2,1)}, u32[]{:S(2)}, u32[]{:S(2)}) collective-permute-start(bf16[88,4096]{1,0:T(8,128)(2,1)} %bitcast.122), channel_id=1, source_target_pairs={{0,1},{1,0},{2,3},{3,2},{4,5},{5,4},{6,7},{7,6},{8,9},{9,8},{10,11... | collective-permute-start | bytes 2162696 | tf_op jit(solution)/shard_map/ppermute | solution.py:27
  56.0 2.4 collective-permute-start.3
  56.0 3.6 %collective-permute-start = (bf16[88,4096]{1,0:T(8,128)(2,1)S(1)}, bf16[88,4096]{1,0:T(8,128)(2,1)}, u32[]{:S(2)}, u32[]{:S(2)}) collective-permute-start(bf16[88,4096]{1,0:T(8,128)(2,1)S(1)} %copy-done.16), channel_id=1, source_target_pairs={{0,1},{1,0},{2,3},{3,2},{4,5},{5,4},{6,7},{7,6},{8,9},{9,8},{10,11... | collective-permute-start | bytes 2162696 | tf_op jit(solution)/shard_map/ppermute | solution.py:27
  62.3 36.5 %copy-start.7 = (bf16[512,32]{0,1:T(8,128)(2,1)S(1)}, bf16[512,32]{0,1:T(8,128)(2,1)}, u32[]{:S(2)}) copy-start(bf16[512,32]{0,1:T(8,128)(2,1)} %param.18) | copy-start | bytes 98308
  62.3 48.6 %copy-start.8 = (bf16[256,256]{1,0:T(8,128)(2,1)S(1)}, bf16[256,256]{1,0:T(8,128)(2,1)}, u32[]{:S(2)}) copy-start(bf16[256,256]{1,0:T(8,128)(2,1)} %param.26) | copy-start | bytes 393220
  62.3 48.9 %copy-start.9 = (bf16[256,256]{1,0:T(8,128)(2,1)S(1)}, bf16[256,256]{1,0:T(8,128)(2,1)}, u32[]{:S(2)}) copy-start(bf16[256,256]{1,0:T(8,128)(2,1)} %param.27) | copy-start | bytes 393220
  62.3 49.2 %copy-start.10 = (bf16[256,256]{1,0:T(8,128)(2,1)S(1)}, bf16[256,256]{1,0:T(8,128)(2,1)}, u32[]{:S(2)}) copy-start(bf16[256,256]{1,0:T(8,128)(2,1)} %param.28) | copy-start | bytes 393220
  99.6 10.9 %all-to-all-start.2 = ((bf16[8,32,512]{2,1,0:T(8,128)(2,1)}), bf16[8,32,512]{2,1,0:T(8,128)(2,1)S(1)}, u32[]{:S(2)}, u32[]{:S(2)}) async-start(bf16[8,32,512]{2,1,0:T(8,128)(2,1)} %broadcast_in_dim.68), calls=%async_computation.2 | async-start | bytes 524288 | tf_op jit(solution)/shard_map/all_to_all | solution.py:19
  110.6 6.5 %copy-start.14 = (f32[256]{0:T(256)S(1)}, f32[256]{0:T(256)}, u32[]{:S(2)}) copy-start(f32[256]{0:T(256)} %param.29) | copy-start | bytes 3076
  113.3 24.4 %all-to-all-start.3 = ((bf16[16,32,1280]{2,1,0:T(8,128)(2,1)}), bf16[16,32,1280]{2,1,0:T(8,128)(2,1)S(1)}, u32[]{:S(2)}, u32[]{:S(2)}) async-start(bf16[16,32,1280]{2,1,0:T(8,128)(2,1)} %bitcast.15), calls=%async_computation.3 | async-start | bytes 2621440 | tf_op jit(solution)/shard_map/all_to_all | solution.py:23
  142.7 17.9 %copy-start.11 = (bf16[256,256]{1,0:T(8,128)(2,1)S(1)}, bf16[256,256]{1,0:T(8,128)(2,1)}, u32[]{:S(2)}) copy-start(bf16[256,256]{1,0:T(8,128)(2,1)} %param.31) | copy-start | bytes 393220
  148.7 28.6 %copy-start.5 = (bf16[4096,88]{0,1:T(8,128)(2,1)S(1)}, bf16[4096,88]{0,1:T(8,128)(2,1)}, u32[]{:S(2)}) copy-start(bf16[4096,88]{0,1:T(8,128)(2,1)} %param.33) | copy-start | bytes 2162692
  172.5 34.6 %all-to-all-start.6 = ((bf16[64,32,512]{2,1,0:T(8,128)(2,1)}), bf16[64,32,512]{2,1,0:T(8,128)(2,1)S(1)}, u32[]{:S(2)}, u32[]{:S(2)}) async-start(bf16[64,32,512]{2,1,0:T(8,128)(2,1)} %broadcast_in_dim.72), calls=%async_computation.6 | async-start | bytes 4194304 | tf_op jit(solution)/shard_map/all_to_all | solution.py:19
  177.2 30.5 %copy-start.13 = (f32[4096]{0:T(1024)S(1)}, f32[4096]{0:T(1024)}, u32[]{:S(2)}) copy-start(f32[4096]{0:T(1024)} %param.32) | copy-start | bytes 49156
  177.2 34.1 %collective-permute-start.5 = (bf16[88,4096]{1,0:T(8,128)(2,1)S(1)}, bf16[88,4096]{1,0:T(8,128)(2,1)}, u32[]{:S(2)}, u32[]{:S(2)}) collective-permute-start(bf16[88,4096]{1,0:T(8,128)(2,1)S(1)} %bitcast.123), channel_id=1, source_target_pairs={{0,1},{1,0},{2,3},{3,2},{4,5},{5,4},{6,7},{7,6},{8,9},{9,8},{10,11... | collective-permute-start | bytes 2162696 | tf_op jit(solution)/shard_map/ppermute | solution.py:27
  177.3 36.0 %collective-permute-start.6 = (bf16[88,4096]{1,0:T(8,128)(2,1)}, bf16[88,4096]{1,0:T(8,128)(2,1)}, u32[]{:S(2)}, u32[]{:S(2)}) collective-permute-start(bf16[88,4096]{1,0:T(8,128)(2,1)} %bitcast.124), channel_id=1, source_target_pairs={{0,1},{1,0},{2,3},{3,2},{4,5},{5,4},{6,7},{7,6},{8,9},{9,8},{10,11... | collective-permute-start | bytes 2162696 | tf_op jit(solution)/shard_map/ppermute | solution.py:27
  215.3 2.3 collective-permute-start.7
  215.4 3.2 %collective-permute-start.4 = (bf16[88,4096]{1,0:T(8,128)(2,1)S(1)}, bf16[88,4096]{1,0:T(8,128)(2,1)S(1)}, u32[]{:S(2)}, u32[]{:S(2)}) collective-permute-start(bf16[88,4096]{1,0:T(8,128)(2,1)S(1)} %copy-done.17), channel_id=1, source_target_pairs={{0,1},{1,0},{2,3},{3,2},{4,5},{5,4},{6,7},{7,6},{8,9},{9,8},{10,11... | collective-permute-start | bytes 2162696 | tf_op jit(solution)/shard_map/ppermute | solution.py:27
  219.9 37.2 %copy-start.1 = (bf16[256,256]{1,0:T(8,128)(2,1)S(1)}, bf16[256,256]{1,0:T(8,128)(2,1)}, u32[]{:S(2)}) copy-start(bf16[256,256]{1,0:T(8,128)(2,1)} %param.25) | copy-start | bytes 393220
  (6 other events, 21.2 us)
